TPU v7x, 32 devices: a whole 2x2x4 slice. The times are simulated.
32 devices in a mesh: grp: 2 (over y), row: 4 (over z), col: 4 (over x, core).
Axes of the slice: x: 2, y: 2, z: 4, core: 2. Of those that a mesh axis runs over, the one named last changes fastest.
Arguments:
- tokens: bfloat16 [5120, 2048], P(('grp', 'row')), parts along dimension 0, may hold values from -6 to 6
- w_four: bfloat16 [2048, 1024], P(None, 'col'), may hold values from -0.125 to 0.125
- w_gate: bfloat16 [2048, 2048], P(None, 'col'), may hold values from -0.125 to 0.125
- w_back: bfloat16 [1024, 2048], P(None, 'col'), may hold values from -0.1875 to 0.1875
Outputs:
- mixed: bfloat16 [5120, 2048], P(('grp', 'row'), 'col'), parts along dimension 0
There are 2 independent parts, one for each index of `grp`. A program takes and returns all parts, laid end to end along the dimension named above; an argument that names none is the same for every part. Nothing has to cross between parts.
All inputs are finite; a program needn't handle non-finite values.
Results may differ from a plain program's by a relative error of at most 0.0085.
Values may be sent and summed in bfloat16 or wider, within the bound.
A program may use at most 64 MiB of HBM per device.

v0:
```python
import math
import jax
import jax.numpy as jnp
from jax import lax
from jax.sharding import PartitionSpec as P

GROUP_DIM = 128


def tables(count_len):
    steps = lax.iota(jnp.int32, count_len)
    product = steps[:, None] * steps[None, :] % count_len
    angles = product.astype(jnp.float32) * (2.0 * math.pi / count_len)
    return (jnp.cos(angles), jnp.sin(angles))


def channel_mix(values, matrix):
    height = values.shape[0]
    shaped = values.reshape(height, -1, GROUP_DIM)
    mixed_ch = jnp.einsum("ngc,cj->ngj", shaped, matrix, precision=lax.Precision.HIGHEST)
    return mixed_ch.reshape(height, -1)


def across_rows(values, matrix):
    return jnp.einsum("kr,rmc->kmc", matrix, values, precision=lax.Precision.HIGHEST)


def long_transform(col_re, col_im):
    length = col_re.shape[0]
    first_len = 8
    second_len = length // first_len
    shaped_re = col_re.reshape(first_len, second_len, -1)
    shaped_im = col_im.reshape(first_len, second_len, -1)
    cos_first, sin_first = tables(first_len)
    cos_second, sin_second = tables(second_len)
    section_re = across_rows(shaped_re, cos_first) + across_rows(shaped_im, sin_first)
    section_im = across_rows(shaped_im, cos_first) - across_rows(shaped_re, sin_first)
    outer = lax.iota(jnp.int32, first_len)[:, None]
    inner = lax.iota(jnp.int32, second_len)[None, :]
    angle = (outer * inner % length).astype(jnp.float32) * (2.0 * math.pi / length)
    turn_cos = jnp.cos(angle)[:, :, None]
    turn_sin = jnp.sin(angle)[:, :, None]
    bent_re = section_re * turn_cos + section_im * turn_sin
    bent_im = section_im * turn_cos - section_re * turn_sin
    final_re = jnp.einsum("qb,kbc->qkc", cos_second, bent_re, precision=lax.Precision.HIGHEST)
    final_re = final_re + jnp.einsum(
        "qb,kbc->qkc", sin_second, bent_im, precision=lax.Precision.HIGHEST
    )
    final_re = final_re.reshape(length, -1)
    final_im = jnp.einsum("qb,kbc->qkc", cos_second, bent_im, precision=lax.Precision.HIGHEST)
    final_im = final_im - jnp.einsum(
        "qb,kbc->qkc", sin_second, bent_re, precision=lax.Precision.HIGHEST
    )
    return (final_re, final_im.reshape(length, -1))


def on_device(tokens, w_four, w_gate, w_back):
    length = tokens.shape[0]
    row_count = lax.axis_size("row")
    row_index = lax.axis_index("row")
    piece_rows = length // row_count
    total_len = length * row_count
    feats = jnp.dot(tokens, w_four, preferred_element_type=jnp.float32).astype(jnp.bfloat16)
    lifted = feats.astype(jnp.float32)
    cos_group, sin_group = tables(GROUP_DIM)
    cos_rows, sin_rows = tables(row_count)
    residue = lax.iota(jnp.int32, row_count)[:, None]
    within = row_index * piece_rows + lax.iota(jnp.int32, piece_rows)[None, :]
    twist = (residue * within % total_len).astype(jnp.float32) * (2.0 * math.pi / total_len)
    twist_cos = jnp.cos(twist)[:, :, None]
    twist_sin = jnp.sin(twist)[:, :, None]
    line_re = lax.all_to_all(
        lifted[None].astype(jnp.bfloat16), "row", split_axis=1, concat_axis=0, tiled=True
    ).astype(jnp.float32)
    freq_re = across_rows(line_re, cos_rows)
    freq_im = -across_rows(line_re, sin_rows)
    turned_re = freq_re * twist_cos + freq_im * twist_sin
    turned_im = freq_im * twist_cos - freq_re * twist_sin
    col_re, col_im = (
        lax.all_to_all(turned_re, "row", split_axis=0, concat_axis=1, tiled=True),
        lax.all_to_all(turned_im, "row", split_axis=0, concat_axis=1, tiled=True),
    )
    col_re = col_re.reshape(length, -1)
    col_im = col_im.reshape(length, -1)
    whole_re, whole_im = long_transform(col_re, col_im)
    result = channel_mix(whole_re, cos_group) + channel_mix(whole_im, sin_group)
    scaled = (result * (1.0 / math.sqrt(total_len * GROUP_DIM))).astype(jnp.bfloat16)
    ordered = lax.all_to_all(scaled[:, None], "row", split_axis=0, concat_axis=1, tiled=True)
    ordered = ordered.reshape(length, -1)
    proj = jnp.dot(
        lax.all_gather(ordered, "col", axis=1, tiled=True),
        w_back,
        preferred_element_type=jnp.float32,
    )
    gate = jax.nn.sigmoid(jnp.dot(tokens, w_gate, preferred_element_type=jnp.float32))
    return (gate * proj).astype(jnp.bfloat16)


def solution(mesh):
    return jax.shard_map(
        on_device,
        mesh=mesh,
        in_specs=(P(("grp", "row"), None), P(None, "col"), P(None, "col"), P(None, "col")),
        out_specs=P(("grp", "row"), "col"),
        check_vma=False,
    )
```

profile of v0, /device:TPU:0, one launch (start us, length us, event | category | flops | bytes accessed | tf_op | source)
XLA Modules:
  0.0 142.1 jit_solution(10061951131345919692)
XLA Ops:
  6.5 1.7 %copy-done = bf16[640,2048]{1,0:T(8,128)(2,1)S(1)} copy-done((bf16[640,2048]{1,0:T(8,128)(2,1)S(1)}, bf16[640,2048]{1,0:T(8,128)(2,1)}, u32[]{:S(2)}) %copy-start) | copy-done | bytes 2621464
  8.3 2.1 %fusion.6 = bf16[1,640,256]{2,1,0:T(8,128)(2,1)S(1)} fusion(bf16[640,2048]{1,0:T(8,128)(2,1)S(1)} %copy-done, bf16[2048,256]{1,0:T(8,128)(2,1)} %param.5), kind=kOutput, calls=%fused_computation.15 | convolution fusion | flops 671252480 | bytes 3997696 | tf_op jit(solution)/shard_map/dot_general | solution.py:63
  11.4 3.3 %reduce = bf16[640,256]{1,0:T(8,128)(2,1)} reduce(bf16[640,1,256]{2,1,0:T(2,128)(2,1)S(1)} %bitcast.61, bf16[]{:T(256)} %broadcast.193), dimensions={1}, to_apply=%bitcast.56.reduce_sub_computation | reduce | bytes 655362
  14.7 1.8 %reshape.136 = bf16[4,2,20480]{2,1,0:T(2,128)(2,1)} reshape(bf16[640,256]{1,0:T(8,128)(2,1)} %reduce) | data formatting | bytes 655360
  16.5 6.3 %all-to-all-start = ((bf16[4,2,20480]{2,1,0:T(2,128)(2,1)}), bf16[4,2,20480]{2,1,0:T(2,128)(2,1)}, u32[]{:S(2)}, u32[]{:S(2)}) async-start(bf16[4,2,20480]{2,1,0:T(2,128)(2,1)} %reshape.136), calls=%async_computation | async-start | bytes 655360 | tf_op jit(solution)/shard_map/all_to_all | solution.py:72
  23.2 10.1 %all-to-all-done = bf16[4,2,20480]{2,1,0:T(2,128)(2,1)} async-done(((bf16[4,2,20480]{2,1,0:T(2,128)(2,1)}), bf16[4,2,20480]{2,1,0:T(2,128)(2,1)}, u32[]{:S(2)}, u32[]{:S(2)}) %all-to-all-start) | async-done | bytes 327712 | tf_op jit(solution)/shard_map/all_to_all | solution.py:72
  33.3 1.2 reshape.137
  35.3 2.0 %multiply_add_fusion.1 = (f32[4,160,256]{2,0,1:T(4,128)S(1)}, f32[4,160,256]{2,0,1:T(4,128)}) fusion(f32[4,160,256]{2,0,1:T(4,128)S(1)} %fusion.23, f32[4,160]{0,1:T(8,128)S(1)} %copy.69, f32[4,160]{0,1:T(8,128)S(1)} %copy.67, bf16[4,160,256]{2,1,0:T(8,128)(2,1)S(1)} %bitcast.65), kind=kOutput, calls=%fused_computation.22 | convolution fusion | flops 9011424 | bytes 2298880 | tf_op jit(solution)/shard_map/kr,rmc->kmc/dot_general | solution.py:25
  37.3 1.0 copy.70
  38.3 3.5 %all-to-all-start.1 = ((f32[4,160,256]{2,1,0:T(8,128)}), f32[4,160,256]{2,1,0:T(8,128)S(1)}, u32[]{:S(2)}, u32[]{:S(2)}) async-start(f32[4,160,256]{2,1,0:T(8,128)} %copy.70), calls=%async_computation.1 | async-start | bytes 1310720 | tf_op jit(solution)/shard_map/all_to_all | solution.py:80
  41.8 2.1 %copy.72 = f32[4,160,256]{2,1,0:T(8,128)} copy(f32[4,160,256]{2,0,1:T(4,128)} %get-tuple-element.6) | data formatting | bytes 1310720 | tf_op jit(solution)/shard_map/sub | solution.py:78
  43.9 13.6 %all-to-all-done.1 = f32[4,160,256]{2,1,0:T(8,128)S(1)} async-done(((f32[4,160,256]{2,1,0:T(8,128)}), f32[4,160,256]{2,1,0:T(8,128)S(1)}, u32[]{:S(2)}, u32[]{:S(2)}) %all-to-all-start.1) | async-done | bytes 655392 | tf_op jit(solution)/shard_map/all_to_all | solution.py:80
  58.3 3.5 %all-to-all-start.2 = ((f32[4,160,256]{2,1,0:T(8,128)}), f32[4,160,256]{2,1,0:T(8,128)S(1)}, u32[]{:S(2)}, u32[]{:S(2)}) async-start(f32[4,160,256]{2,1,0:T(8,128)} %copy.72), calls=%async_computation.2 | async-start | bytes 1310720 | tf_op jit(solution)/shard_map/all_to_all | solution.py:81
  62.3 2.9 %fusion.20 = f32[8,80,256]{2,0,1:T(8,128)} fusion(f32[8,80,256]{2,1,0:T(8,128)} %bitcast.59), kind=kOutput, calls=%fused_computation.33 | convolution fusion | flops 15729536 | bytes 1310720 | tf_op jit(solution)/shard_map/kr,rmc->kmc/dot_general | solution.py:25
  65.2 13.1 %all-to-all-done.2 = f32[4,160,256]{2,1,0:T(8,128)S(1)} async-done(((f32[4,160,256]{2,1,0:T(8,128)}), f32[4,160,256]{2,1,0:T(8,128)S(1)}, u32[]{:S(2)}, u32[]{:S(2)}) %all-to-all-start.2) | async-done | bytes 655392 | tf_op jit(solution)/shard_map/all_to_all | solution.py:81
  78.3 1.0 fusion.16
  79.4 1.0 convolution_subtract_fusion.1
  80.5 1.2 multiply_subtract_fusion
  81.7 1.0 fusion.10
  83.6 1.8 %convolution_subtract_fusion = f32[80,8,256]{2,0,1:T(8,128)} fusion(f32[80,8,256]{2,0,1:T(8,128)S(1)} %fusion.10, f32[8,80,256]{2,0,1:T(8,128)S(1)} %get-tuple-element.8), kind=kOutput, calls=%fused_computation.7 | convolution fusion | flops 157507840 | bytes 1966080 | tf_op jit(solution)/shard_map/qb,kbc->qkc/dot_general | solution.py:51
  85.5 1.0 convolution_add_fusion.1
  86.8 1.2 reshape_reshape.14
  88.0 2.1 %fusion.8 = f32[640,2,128]{0,2,1:T(8,128)S(1)} fusion(f32[640,2,128]{2,1,0:T(2,128)} %reshape_reshape.14), kind=kOutput, calls=%fused_computation.17 | convolution fusion | flops 251887616 | bytes 1310720 | tf_op jit(solution)/shard_map/ngc,cj->ngj/dot_general | solution.py:20
  90.1 1.2 copy.84
  91.4 2.3 %reshape_reshape.15 = f32[640,2,128]{2,1,0:T(2,128)} reshape(f32[80,8,256]{2,1,0:T(8,128)} %copy.84) | data formatting | bytes 1310720 | tf_op jit(solution)/shard_map/reshape;reshape | solution.py:19
  93.6 2.8 %fusion.5 = bf16[640,2,128]{0,2,1:T(8,128)(2,1)} fusion(f32[640,2,128]{0,2,1:T(8,128)S(1)} %fusion.8, f32[640,2,128]{2,1,0:T(2,128)} %reshape_reshape.15), kind=kOutput, calls=%fused_computation.13 | convolution fusion | flops 252379136 | bytes 1638400 | tf_op jit(solution)/shard_map/ngc,cj->ngj/dot_general | solution.py:20
  96.4 1.8 %reduce.1 = bf16[640,256]{0,1:T(8,128)(2,1)S(1)} reduce(bf16[640,1,256]{0,2,1:T(8,128)(2,1)} %bitcast.66, bf16[]{:T(256)} %broadcast.193), dimensions={1}, to_apply=%copy.86.reduce_sub_computation | reduce | bytes 655362 | tf_op jit(solution)/shard_map/convert_element_type | solution.py:87
  98.6 12.9 %all_to_all.45 = bf16[4,2,20480]{2,1,0:T(2,128)(2,1)} all-to-all(bf16[4,2,20480]{2,1,0:T(2,128)(2,1)S(1)} %reshape.138), channel_id=1, replica_groups=mesh['grp'=2,'row'=4,'col'=4] {'row'}, dimensions={0} | all-to-all | bytes 655360 | tf_op jit(solution)/shard_map/all_to_all | solution.py:88
  111.6 1.2 reshape.139
  114.0 4.3 %fusion.2 = f32[640,512]{1,0:T(8,128)} fusion(bf16[640,2048]{1,0:T(8,128)(2,1)S(1)} %copy-done, bf16[2048,512]{1,0:T(8,128)(2,1)} %param.6), kind=kOutput, calls=%fused_computation.4 | convolution fusion | flops 1343160320 | bytes 6029312 | tf_op jit(solution)/shard_map/dot_general | solution.py:95
  118.3 13.2 %all-gather.2.cloned.1.call-done = bf16[640,1024]{1,0:T(8,128)(2,1)} async-done(((bf16[640,256]{1,0:T(8,128)(2,1)}), bf16[640,1024]{1,0:T(8,128)(2,1)}) %all-gather.2.cloned.1.call-update) | async-done | bytes 1310736 | tf_op jit(solution)/shard_map/all_gather | solution.py:91
  131.5 3.7 %fusion.3 = bf16[640,512]{1,0:T(8,128)(2,1)} fusion(f32[640,512]{1,0:T(8,128)} %fusion.2, bf16[640,1024]{1,0:T(8,128)(2,1)} %all-gather.2.cloned.1.call-done, bf16[1024,512]{1,0:T(8,128)(2,1)} %param.7), kind=kOutput, calls=%fused_computation.5 | convolution fusion | flops 671744000 | bytes 4325376 | tf_op jit(solution)/shard_map/dot_general | solution.py:90
  (30 shorter events, 6.6 us)
Async XLA Ops:
  6.5 1.7 %copy-start = (bf16[640,2048]{1,0:T(8,128)(2,1)S(1)}, bf16[640,2048]{1,0:T(8,128)(2,1)}, u32[]{:S(2)}) copy-start(bf16[640,2048]{1,0:T(8,128)(2,1)} %param.4) | copy-start | bytes 7864324
  16.5 16.8 %all-to-all-start = ((bf16[4,2,20480]{2,1,0:T(2,128)(2,1)}), bf16[4,2,20480]{2,1,0:T(2,128)(2,1)}, u32[]{:S(2)}, u32[]{:S(2)}) async-start(bf16[4,2,20480]{2,1,0:T(2,128)(2,1)} %reshape.136), calls=%async_computation | async-start | bytes 655360 | tf_op jit(solution)/shard_map/all_to_all | solution.py:72
  38.3 19.1 %all-to-all-start.1 = ((f32[4,160,256]{2,1,0:T(8,128)}), f32[4,160,256]{2,1,0:T(8,128)S(1)}, u32[]{:S(2)}, u32[]{:S(2)}) async-start(f32[4,160,256]{2,1,0:T(8,128)} %copy.70), calls=%async_computation.1 | async-start | bytes 1310720 | tf_op jit(solution)/shard_map/all_to_all | solution.py:80
  57.4 0.8 copy-start.1
  58.3 20.0 %all-to-all-start.2 = ((f32[4,160,256]{2,1,0:T(8,128)}), f32[4,160,256]{2,1,0:T(8,128)S(1)}, u32[]{:S(2)}, u32[]{:S(2)}) async-start(f32[4,160,256]{2,1,0:T(8,128)} %copy.72), calls=%async_computation.2 | async-start | bytes 1310720 | tf_op jit(solution)/shard_map/all_to_all | solution.py:81
  61.8 69.8 %all-gather.2.cloned.1.call-start = ((), (), s32[]{:S(2)}) async-start(), calls=%async_computation.4 | async-start | bytes 1638400 | tf_op jit(solution)/shard_map/all_gather | solution.py:91
  78.3 1.1 copy-start.2
  79.4 1.1 copy-start.3
  88.0 2.1 %copy-start.4 = (f32[80,8,256]{2,0,1:T(8,128)S(1)}, f32[80,8,256]{2,0,1:T(8,128)}, u32[]{:S(2)}) copy-start(f32[80,8,256]{2,0,1:T(8,128)} %convolution_subtract_fusion) | copy-start | bytes 1966084
Sparse Core Ops, SparseCore 0:
  114.1 17.4 all-gather.1
where the time goes:
time: 143 us; the launch traced here: 142 us
  waiting for transfers between devices  50 us (35%)
  matrix products  28.6 us (20%)
  local copies, waits for them, and re-layouts  18.2 us (13%)
  between operations  13.6 us (10%)
  starting transfers between devices  13.5 us (9%)
  blocking collectives  12.9 us (9%)
  other arithmetic  5.24 us (4%)
    all_to_all x1, waiting for transfers between devices, on_device(): lax.all_to_all(turned_re, 'row', split_axis=0, concat_axis=1, tiled=True)  13.6 us
    all_gather x1, waiting for transfers between devices, on_device(): lax.all_gather(ordered, 'col', axis=1, tiled=True)  13.2 us
    all_to_all x1, waiting for transfers between devices, on_device(): lax.all_to_all(turned_im, 'row', split_axis=0, concat_axis=1, tiled=True)  13.1 us
    all_to_all x1, blocking collectives, on_device(): lax.all_to_all(scaled[:, None], 'row', split_axis=0, concat_axis=1, tiled...  12.9 us
    all_to_all x1, waiting for transfers between devices, on_device(): lax.all_to_all(lifted[None].astype(jnp.bfloat16), 'row', split_axis=1, co...  10.1 us
    dot_general x6, matrix products, across_rows(): jnp.einsum('kr,rmc->kmc', matrix, values, precision=lax.Precision.HIGHEST)  8.85 us
    unnamed x18, local copies, waits for them, and re-layouts  8.15 us
    all_to_all x1, starting transfers between devices, on_device(): lax.all_to_all(lifted[None].astype(jnp.bfloat16), 'row', split_axis=1, co...  6.35 us
  transfers between devices with their start and end apart: 4, of which 4 were waited for; matrix products, arithmetic and copies ran while one was open for 7% of the time, Pallas kernels for 0%

commit v1 on v0

--- a/solution.py
+++ b/solution.py
@@ -1,3 +1,4 @@
+import functools
 import math
 import jax
 import jax.numpy as jnp
@@ -5,6 +6,15 @@
 from jax.sharding import PartitionSpec as P
 
 GROUP_DIM = 128
+
+
+def shape_the_unit(my_tile, join_dim, ndim_at):
+    tall = lax.axis_size("row")
+    moved = jnp.stack(jnp.split(my_tile, tall, axis=join_dim))
+    return jnp.concatenate(lax.all_to_all(moved, "row", 0, 0), axis=ndim_at)
+
+
+_report_patches = functools.partial(shape_the_unit, join_dim=1, ndim_at=0)
 
 
 def tables(count_len):
@@ -69,9 +79,7 @@
     twist = (residue * within % total_len).astype(jnp.float32) * (2.0 * math.pi / total_len)
     twist_cos = jnp.cos(twist)[:, :, None]
     twist_sin = jnp.sin(twist)[:, :, None]
-    line_re = lax.all_to_all(
-        lifted[None].astype(jnp.bfloat16), "row", split_axis=1, concat_axis=0, tiled=True
-    ).astype(jnp.float32)
+    line_re = _report_patches(lifted[None].astype(jnp.bfloat16)).astype(jnp.float32)
     freq_re = across_rows(line_re, cos_rows)
     freq_im = -across_rows(line_re, sin_rows)
     turned_re = freq_re * twist_cos + freq_im * twist_sin

time: 143 us -> 137 us (0.958)
  local copies, waits for them, and re-layouts: 18.2 us -> 14.4 us
  other arithmetic: 5.24 us -> 2.7 us
    unnamed x18 -> x14, local copies, waits for them, and re-layouts: 8.15 us -> 4.29 us
    unnamed x1 -> x0, other arithmetic: 3.31 us -> none
where the time goes in v1:
time: 137 us; the launch traced here: 136 us
  waiting for transfers between devices  49.9 us (36%)
  matrix products  28.6 us (21%)
  local copies, waits for them, and re-layouts  14.4 us (11%)
  between operations  13.8 us (10%)
  starting transfers between devices  13.5 us (10%)
  blocking collectives  12.9 us (9%)
  other arithmetic  2.7 us (2%)
    all_to_all x1, waiting for transfers between devices, on_device(): lax.all_to_all(turned_re, 'row', split_axis=0, concat_axis=1, tiled=True)  13.6 us
    all_gather x1, waiting for transfers between devices, on_device(): lax.all_gather(ordered, 'col', axis=1, tiled=True)  13.2 us
    all_to_all x1, waiting for transfers between devices, on_device(): lax.all_to_all(turned_im, 'row', split_axis=0, concat_axis=1, tiled=True)  13.1 us
    all_to_all x1, blocking collectives, on_device(): lax.all_to_all(scaled[:, None], 'row', split_axis=0, concat_axis=1, tiled...  12.9 us
    all_to_all x1, waiting for transfers between devices, shape_the_unit(): return jnp.concatenate(lax.all_to_all(moved, 'row', 0, 0), axis=ndim_at)  10 us
    dot_general x6, matrix products, across_rows(): jnp.einsum('kr,rmc->kmc', matrix, values, precision=lax.Precision.HIGHEST)  8.87 us
    all_to_all x1, starting transfers between devices, shape_the_unit(): return jnp.concatenate(lax.all_to_all(moved, 'row', 0, 0), axis=ndim_at)  6.35 us
    dot_general x2, matrix products, channel_mix(): jnp.einsum('ngc,cj->ngj', shaped, matrix, precision=lax.Precision.HIGHEST)  4.93 us
  transfers between devices with their start and end apart: 4, of which 4 were waited for; matrix products, arithmetic and copies ran while one was open for 7% of the time, Pallas kernels for 0%

profile of v1, /device:TPU:0, one launch (start us, length us, event | category | flops | bytes accessed | tf_op | source)
XLA Modules:
  0.0 135.9 jit_solution(8198326035737303416)
XLA Ops:
  6.5 1.7 %copy-done = bf16[640,2048]{1,0:T(8,128)(2,1)S(1)} copy-done((bf16[640,2048]{1,0:T(8,128)(2,1)S(1)}, bf16[640,2048]{1,0:T(8,128)(2,1)}, u32[]{:S(2)}) %copy-start) | copy-done | bytes 2621464
  8.3 2.1 %fusion.6 = bf16[1,640,256]{2,1,0:T(8,128)(2,1)S(1)} fusion(bf16[640,2048]{1,0:T(8,128)(2,1)S(1)} %copy-done, bf16[2048,256]{1,0:T(8,128)(2,1)} %param.5), kind=kOutput, calls=%fused_computation.15 | convolution fusion | flops 671252480 | bytes 3997696 | tf_op jit(solution)/shard_map/dot_general | solution.py:73
  11.1 6.3 %all-to-all-start = ((bf16[4,1,160,256]{3,2,1,0:T(8,128)(2,1)}), bf16[4,1,160,256]{3,2,1,0:T(8,128)(2,1)S(1)}, u32[]{:S(2)}, u32[]{:S(2)}) async-start(bf16[4,1,160,256]{3,2,1,0:T(8,128)(2,1)} %pad_maximum_fusion), calls=%async_computation | async-start | bytes 655360 | tf_op jit(solution)/shard_map/all_to_all | solution.py:14
  17.8 10.0 %all-to-all-done = bf16[4,1,160,256]{3,2,1,0:T(8,128)(2,1)S(1)} async-done(((bf16[4,1,160,256]{3,2,1,0:T(8,128)(2,1)}), bf16[4,1,160,256]{3,2,1,0:T(8,128)(2,1)S(1)}, u32[]{:S(2)}, u32[]{:S(2)}) %all-to-all-start) | async-done | bytes 327712 | tf_op jit(solution)/shard_map/all_to_all | solution.py:14
  28.5 2.0 %multiply_add_fusion.1 = (f32[4,160,256]{2,0,1:T(4,128)S(1)}, f32[4,160,256]{2,0,1:T(4,128)}) fusion(f32[4,160,256]{2,0,1:T(4,128)S(1)} %fusion.23, f32[4,160]{0,1:T(8,128)S(1)} %copy.50, f32[4,160]{0,1:T(8,128)S(1)} %copy.48, bf16[4,160,256]{2,1,0:T(8,128)(2,1)S(1)} %bitcast.66), kind=kOutput, calls=%fused_computation.22 | convolution fusion | flops 9011424 | bytes 2298880 | tf_op jit(solution)/shard_map/kr,rmc->kmc/dot_general | solution.py:35
  30.6 1.0 copy.51
  31.5 3.5 %all-to-all-start.1 = ((f32[4,160,256]{2,1,0:T(8,128)}), f32[4,160,256]{2,1,0:T(8,128)S(1)}, u32[]{:S(2)}, u32[]{:S(2)}) async-start(f32[4,160,256]{2,1,0:T(8,128)} %copy.51), calls=%async_computation.1 | async-start | bytes 1310720 | tf_op jit(solution)/shard_map/all_to_all | solution.py:88
  35.0 2.1 %copy.53 = f32[4,160,256]{2,1,0:T(8,128)} copy(f32[4,160,256]{2,0,1:T(4,128)} %get-tuple-element.6) | data formatting | bytes 1310720 | tf_op jit(solution)/shard_map/sub | solution.py:86
  37.1 13.6 %all-to-all-done.1 = f32[4,160,256]{2,1,0:T(8,128)S(1)} async-done(((f32[4,160,256]{2,1,0:T(8,128)}), f32[4,160,256]{2,1,0:T(8,128)S(1)}, u32[]{:S(2)}, u32[]{:S(2)}) %all-to-all-start.1) | async-done | bytes 655392 | tf_op jit(solution)/shard_map/all_to_all | solution.py:88
  50.7 0.8 copy-done.1
  51.5 3.5 %all-to-all-start.2 = ((f32[4,160,256]{2,1,0:T(8,128)}), f32[4,160,256]{2,1,0:T(8,128)S(1)}, u32[]{:S(2)}, u32[]{:S(2)}) async-start(f32[4,160,256]{2,1,0:T(8,128)} %copy.53), calls=%async_computation.2 | async-start | bytes 1310720 | tf_op jit(solution)/shard_map/all_to_all | solution.py:89
  55.5 3.0 %fusion.20 = f32[8,80,256]{2,0,1:T(8,128)} fusion(f32[8,80,256]{2,1,0:T(8,128)} %bitcast.63), kind=kOutput, calls=%fused_computation.33 | convolution fusion | flops 15729536 | bytes 1310720 | tf_op jit(solution)/shard_map/kr,rmc->kmc/dot_general | solution.py:35
  58.5 13.1 %all-to-all-done.2 = f32[4,160,256]{2,1,0:T(8,128)S(1)} async-done(((f32[4,160,256]{2,1,0:T(8,128)}), f32[4,160,256]{2,1,0:T(8,128)S(1)}, u32[]{:S(2)}, u32[]{:S(2)}) %all-to-all-start.2) | async-done | bytes 655392 | tf_op jit(solution)/shard_map/all_to_all | solution.py:89
  71.6 1.0 fusion.16
  72.6 1.0 convolution_subtract_fusion.1
  73.7 1.2 multiply_subtract_fusion
  74.9 1.0 fusion.10
  75.9 1.0 fusion.14
  76.9 1.8 %convolution_subtract_fusion = f32[80,8,256]{2,0,1:T(8,128)} fusion(f32[80,8,256]{2,0,1:T(8,128)S(1)} %fusion.10, f32[8,80,256]{2,0,1:T(8,128)S(1)} %get-tuple-element.8), kind=kOutput, calls=%fused_computation.7 | convolution fusion | flops 157507840 | bytes 1966080 | tf_op jit(solution)/shard_map/qb,kbc->qkc/dot_general | solution.py:61
  78.7 1.0 convolution_add_fusion.1
  80.1 1.2 reshape_reshape.14
  81.2 2.1 %fusion.8 = f32[640,2,128]{0,2,1:T(8,128)S(1)} fusion(f32[640,2,128]{2,1,0:T(2,128)} %reshape_reshape.14), kind=kOutput, calls=%fused_computation.17 | convolution fusion | flops 251887616 | bytes 1310720 | tf_op jit(solution)/shard_map/ngc,cj->ngj/dot_general | solution.py:30
  83.4 1.2 copy.65
  84.6 2.3 %reshape_reshape.15 = f32[640,2,128]{2,1,0:T(2,128)} reshape(f32[80,8,256]{2,1,0:T(8,128)} %copy.65) | data formatting | bytes 1310720 | tf_op jit(solution)/shard_map/reshape;reshape | solution.py:29
  86.9 2.8 %fusion.5 = bf16[640,2,128]{0,2,1:T(8,128)(2,1)} fusion(f32[640,2,128]{0,2,1:T(8,128)S(1)} %fusion.8, f32[640,2,128]{2,1,0:T(2,128)} %reshape_reshape.15), kind=kOutput, calls=%fused_computation.13 | convolution fusion | flops 252379136 | bytes 1638400 | tf_op jit(solution)/shard_map/ngc,cj->ngj/dot_general | solution.py:30
  90.2 1.8 %reduce = bf16[640,256]{0,1:T(8,128)(2,1)S(1)} reduce(bf16[640,1,256]{0,2,1:T(8,128)(2,1)} %bitcast.68, bf16[]{:T(256)} %broadcast.193), dimensions={1}, to_apply=%copy.67.reduce_sub_computation | reduce | bytes 655362 | tf_op jit(solution)/shard_map/convert_element_type | solution.py:95
  92.5 12.9 %all_to_all.38 = bf16[4,2,20480]{2,1,0:T(2,128)(2,1)} all-to-all(bf16[4,2,20480]{2,1,0:T(2,128)(2,1)S(1)} %reshape.137), channel_id=1, replica_groups=mesh['grp'=2,'row'=4,'col'=4] {'row'}, dimensions={0} | all-to-all | bytes 655360 | tf_op jit(solution)/shard_map/all_to_all | solution.py:96
  105.4 1.2 reshape.138
  106.9 0.8 reshape.128
  107.8 4.4 %fusion.2 = f32[640,512]{1,0:T(8,128)} fusion(bf16[640,2048]{1,0:T(8,128)(2,1)S(1)} %copy-done, bf16[2048,512]{1,0:T(8,128)(2,1)} %param.6), kind=kOutput, calls=%fused_computation.4 | convolution fusion | flops 1343160320 | bytes 6029312 | tf_op jit(solution)/shard_map/dot_general | solution.py:103
  112.1 13.2 %all-gather.2.cloned.1.call-done = bf16[640,1024]{1,0:T(8,128)(2,1)} async-done(((bf16[640,256]{1,0:T(8,128)(2,1)}), bf16[640,1024]{1,0:T(8,128)(2,1)}) %all-gather.2.cloned.1.call-update) | async-done | bytes 1310736 | tf_op jit(solution)/shard_map/all_gather | solution.py:99
  125.3 3.7 %fusion.3 = bf16[640,512]{1,0:T(8,128)(2,1)} fusion(f32[640,512]{1,0:T(8,128)} %fusion.2, bf16[640,1024]{1,0:T(8,128)(2,1)} %all-gather.2.cloned.1.call-done, bf16[1024,512]{1,0:T(8,128)(2,1)} %param.7), kind=kOutput, calls=%fused_computation.5 | convolution fusion | flops 671744000 | bytes 4325376 | tf_op jit(solution)/shard_map/dot_general | solution.py:98
  (27 shorter events, 4.0 us)
Async XLA Ops:
  6.5 1.7 %copy-start = (bf16[640,2048]{1,0:T(8,128)(2,1)S(1)}, bf16[640,2048]{1,0:T(8,128)(2,1)}, u32[]{:S(2)}) copy-start(bf16[640,2048]{1,0:T(8,128)(2,1)} %param.4) | copy-start | bytes 7864324
  11.1 16.7 %all-to-all-start = ((bf16[4,1,160,256]{3,2,1,0:T(8,128)(2,1)}), bf16[4,1,160,256]{3,2,1,0:T(8,128)(2,1)S(1)}, u32[]{:S(2)}, u32[]{:S(2)}) async-start(bf16[4,1,160,256]{3,2,1,0:T(8,128)(2,1)} %pad_maximum_fusion), calls=%async_computation | async-start | bytes 655360 | tf_op jit(solution)/shard_map/all_to_all | solution.py:14
  31.5 19.1 %all-to-all-start.1 = ((f32[4,160,256]{2,1,0:T(8,128)}), f32[4,160,256]{2,1,0:T(8,128)S(1)}, u32[]{:S(2)}, u32[]{:S(2)}) async-start(f32[4,160,256]{2,1,0:T(8,128)} %copy.51), calls=%async_computation.1 | async-start | bytes 1310720 | tf_op jit(solution)/shard_map/all_to_all | solution.py:88
  50.7 0.8 copy-start.1
  51.5 20.0 %all-to-all-start.2 = ((f32[4,160,256]{2,1,0:T(8,128)}), f32[4,160,256]{2,1,0:T(8,128)S(1)}, u32[]{:S(2)}, u32[]{:S(2)}) async-start(f32[4,160,256]{2,1,0:T(8,128)} %copy.53), calls=%async_computation.2 | async-start | bytes 1310720 | tf_op jit(solution)/shard_map/all_to_all | solution.py:89
  55.0 70.3 %all-gather.2.cloned.1.call-start = ((), (), s32[]{:S(2)}) async-start(), calls=%async_computation.4 | async-start | bytes 1638400 | tf_op jit(solution)/shard_map/all_gather | solution.py:99
  71.6 1.1 copy-start.2
  72.6 1.1 copy-start.3
  81.2 2.1 %copy-start.4 = (f32[80,8,256]{2,0,1:T(8,128)S(1)}, f32[80,8,256]{2,0,1:T(8,128)}, u32[]{:S(2)}) copy-start(f32[80,8,256]{2,0,1:T(8,128)} %convolution_subtract_fusion) | copy-start | bytes 1966084
Sparse Core Ops, SparseCore 0:
  107.9 17.4 all-gather.1
